TPU v7x, 128 devices: a whole 4x4x4 slice. The times are simulated.
128 devices in a mesh: kv: 16 (over z, y), tp: 8 (over x, core).
Axes of the slice: x: 4, y: 4, z: 4, core: 2. Of those that a mesh axis runs over, the one named last changes fastest.
Arguments:
- tokens: bfloat16 [320, 4096], P(None, 'kv'), may hold values from -40 to 40
- input_norm_gain: float32 [4096], P('kv'), may hold values from 0.1 to 1.9
- input_matrix: bfloat16 [4096, 4096], P('kv', 'tp'), may hold values from -0.09375 to 0.09375
- gate_matrix: bfloat16 [4096, 4096], P('kv', 'tp'), may hold values from -0.09375 to 0.09375
- write_matrix: bfloat16 [4096, 1024], P('kv', 'tp'), may hold values from -0.09375 to 0.09375
- read_matrix: bfloat16 [4096, 1024], P('kv', 'tp'), may hold values from -0.09375 to 0.09375
- step_matrix: bfloat16 [4096, 64], replicated, may hold values from -0.09375 to 0.09375
- input_kernel: float32 [4, 4096], P(None, 'tp'), may hold values from -3 to 3
- write_kernel: float32 [4, 1024], P(None, 'tp'), may hold values from -3 to 3
- read_kernel: float32 [4, 1024], P(None, 'tp'), may hold values from -3 to 3
- step_size_bias: float32 [64], P('tp'), may hold values from -6 to 1
- head_decay_logs: float32 [64], P('tp'), may hold values from 0 to 2.77
- bypass_scale: float32 [64], P('tp'), may hold values from 0.5 to 1.5
- extra_decay_logs: float32 [320, 64], P('kv', 'tp'), may hold values from -0.7 to 0, as said below
- output_norm_gain: float32 [4096], P('tp'), may hold values from 0.1 to 1.9
- output_matrix: bfloat16 [4096, 4096], P('tp', 'kv'), may hold values from -0.09375 to 0.09375
- cached_state_history: float32 [64, 6, 64, 64, 128], P('kv', None, 'tp'), may hold values from -2 to 2
- cached_input_rows: bfloat16 [64, 8, 4096], P('kv', None, 'tp'), may hold values from -6 to 6
- cached_write_rows: bfloat16 [64, 8, 1024], P('kv', None, 'tp'), may hold values from -6 to 6
- cached_read_rows: bfloat16 [64, 8, 1024], P('kv', None, 'tp'), may hold values from -6 to 6
- accepted: int32 [64], P('kv'), may hold values from 0 to 5
Outputs:
- mixer_out: bfloat16 [320, 4096], P('tp', 'kv')
- next_states: float32 [64, 6, 64, 64, 128], P('kv', None, 'tp')
- next_input: bfloat16 [64, 8, 4096], P('kv', None, 'tp')
- next_write: bfloat16 [64, 8, 1024], P('kv', None, 'tp')
- next_read: bfloat16 [64, 8, 1024], P('kv', None, 'tp')
Inputs may be any that keep to these rules, and one draw needn't show every extreme that they name: `extra_decay_logs`: zero at most tokens and heads.
All inputs are finite; a program needn't handle non-finite values.
Results may differ from a plain program's by a relative error of at most 0.03.
Values may be sent and summed in bfloat16 or wider, within the bound.
No kernel may reach another device: no remote copies, remote signals or barrier semaphores. Data moves between devices by JAX's collectives and lax.ppermute only.
A program may use at most 64 MiB of HBM per device.

v0:
```python
import math

import jax
import jax.numpy as jnp
from jax import lax
from jax.sharding import PartitionSpec as P

D = 4096
HEAD_TOTAL = 64
P_SIZE = 64
N = 128
G = 8
TAPS = 4
DRAFT_TOKENS = 5


epsilon = 1e-05


def in_blocks(value, dim, peers):
    dims = value.shape
    parts = value.reshape(*dims[:dim], peers, dims[dim] // peers, *dims[dim + 1 :])
    return jnp.moveaxis(parts, dim, 0)


def sum_at_owner(value, axis, dim):
    peers = lax.axis_size(axis)
    parts = lax.all_to_all(in_blocks(value, dim, peers), axis, 0, 0, tiled=True)
    return jnp.sum(parts.astype(jnp.float32), axis=0)


def sent_together(arrays, axis, dim, along):
    widths = [math.prod(a.shape[along:]) for a in arrays]
    both = jnp.concatenate(
        [a.reshape(*a.shape[:along], w) for a, w in zip(arrays, widths)], axis=along
    )
    result = sum_at_owner(both, axis, dim)
    parts = jnp.split(result, [sum(widths[:k]) for k in range(1, len(widths))], axis=along)
    return tuple(
        (b.reshape(*result.shape[:along], *a.shape[along:]) for a, b in zip(arrays, parts))
    )


def joined_along(parts, dim):
    dims = list(parts.shape[1:])
    dims[dim] *= parts.shape[0]
    return jnp.moveaxis(parts, 0, dim).reshape(dims)


def copy_for_each(value, axis):
    peers = lax.axis_size(axis)
    return lax.all_to_all(
        jnp.broadcast_to(value[None], (peers, *value.shape)), axis, 0, 0, tiled=True
    )


def gathered_copies(value, axis, dim):
    return joined_along(copy_for_each(value, axis), dim)


def convolve(window, taps):
    total = jnp.zeros((window.shape[0], DRAFT_TOKENS, window.shape[2]), jnp.float32)
    for tap_index in range(TAPS):
        total = total + taps[tap_index] * window[:, tap_index : tap_index + DRAFT_TOKENS].astype(
            jnp.float32
        )
    return jax.nn.silu(total)


def per_device(
    tokens,
    input_norm_gain,
    input_matrix,
    gate_matrix,
    write_matrix,
    read_matrix,
    step_matrix,
    input_kernel,
    write_kernel,
    read_kernel,
    step_size_bias,
    head_decay_logs,
    bypass_scale,
    extra_decay_logs,
    output_norm_gain,
    output_matrix,
    cached_state_history,
    cached_input_rows,
    cached_write_rows,
    cached_read_rows,
    accepted,
):
    kv_count = lax.axis_size("kv")
    own_rows = tokens.shape[0] // kv_count
    local_sequences = own_rows // DRAFT_TOKENS
    local_width = tokens.shape[1]
    local_heads = step_size_bias.shape[0]
    groups_here = write_matrix.shape[1] // N
    input_width = input_matrix.shape[1]
    state_width = write_matrix.shape[1]
    wide_rows = tokens.astype(jnp.float32)
    scaled = (wide_rows * input_norm_gain).astype(jnp.bfloat16)
    weights = (input_matrix, gate_matrix, write_matrix, read_matrix)
    squares = jnp.sum(wide_rows * wide_rows, axis=1)
    step_block = lax.dynamic_slice(
        step_matrix,
        (lax.axis_index("kv") * local_width, lax.axis_index("tp") * local_heads),
        (local_width, local_heads),
    )
    step_term = jnp.dot(scaled, step_block, preferred_element_type=jnp.float32)
    joined, step_raw, square_sums = sent_together(
        (
            jnp.concatenate(
                [jnp.dot(scaled, weight, preferred_element_type=jnp.float32) for weight in weights],
                axis=1,
            ).astype(jnp.bfloat16),
            step_term.astype(jnp.bfloat16),
            squares.astype(jnp.bfloat16),
        ),
        "kv",
        0,
        1,
    )
    inverse = lax.rsqrt(square_sums / D + epsilon)[:, None]
    joined = (joined * inverse).astype(jnp.bfloat16)
    fresh_input = joined[:, :input_width]
    fresh_gate = joined[:, input_width : 2 * input_width]
    fresh_write = joined[:, 2 * input_width : 2 * input_width + state_width]
    fresh_read = joined[:, 2 * input_width + state_width :]
    step_raw = step_raw * inverse
    row_picks = (
        jnp.arange(DRAFT_TOKENS + TAPS - 1, dtype=jnp.int32)[None, None, :]
        == accepted[:, None, None] + jnp.arange(TAPS - 1, dtype=jnp.int32)[None, :, None]
    ).astype(jnp.bfloat16)

    def make_window(saved, fresh):
        taken_rows = jnp.einsum(
            "srj,sjc->src", row_picks, saved, preferred_element_type=jnp.float32
        ).astype(jnp.bfloat16)
        return jnp.concatenate(
            [taken_rows, fresh.reshape(local_sequences, DRAFT_TOKENS, -1)], axis=1
        )

    next_input = make_window(cached_input_rows, fresh_input)
    next_write = make_window(cached_write_rows, fresh_write)
    next_read = make_window(cached_read_rows, fresh_read)
    conv_input = convolve(next_input, input_kernel).reshape(
        local_sequences, DRAFT_TOKENS, local_heads, P_SIZE
    )
    conv_write = jnp.repeat(
        convolve(next_write, write_kernel).reshape(local_sequences, DRAFT_TOKENS, groups_here, N),
        HEAD_TOTAL // G,
        axis=2,
    )
    conv_read = jnp.repeat(
        convolve(next_read, read_kernel).reshape(local_sequences, DRAFT_TOKENS, groups_here, N),
        HEAD_TOTAL // G,
        axis=2,
    )
    step_sizes = jax.nn.softplus(
        step_raw.reshape(local_sequences, DRAFT_TOKENS, local_heads) + step_size_bias
    )
    retain_logs = -step_sizes * jnp.exp(head_decay_logs) + extra_decay_logs.reshape(
        local_sequences, DRAFT_TOKENS, local_heads
    )
    chosen = jnp.arange(DRAFT_TOKENS + 1, dtype=jnp.int32)[None, :] == accepted[:, None]
    carried = jnp.sum(jnp.where(chosen[:, :, None, None, None], cached_state_history, 0.0), axis=1)
    states = [carried]
    outputs = []
    for position in range(DRAFT_TOKENS):
        written = (step_sizes[:, position, :, None] * conv_input[:, position])[:, :, :, None]
        carried = (
            jnp.exp(retain_logs[:, position])[:, :, None, None] * carried
            + written * conv_write[:, position][:, :, None, :]
        )
        states.append(carried)
        outputs.append(
            jnp.sum(carried * conv_read[:, position][:, :, None, :], axis=-1)
            + bypass_scale[:, None] * conv_input[:, position]
        )
    head_out = jnp.stack(outputs, axis=1).reshape(own_rows, input_width)
    gated = (head_out * jax.nn.silu(fresh_gate.astype(jnp.float32))).reshape(
        own_rows, groups_here, -1
    )
    gated = gated * lax.rsqrt(jnp.mean(gated * gated, axis=-1, keepdims=True) + epsilon)
    normed = (gated.reshape(own_rows, input_width) * output_norm_gain).astype(jnp.bfloat16)
    partial_value = jnp.dot(
        gathered_copies(normed, "kv", 0), output_matrix, preferred_element_type=jnp.float32
    )
    mixer_out = sum_at_owner(partial_value.astype(jnp.bfloat16), "tp", 0).astype(jnp.bfloat16)
    next_states = jnp.stack(states, axis=1)
    return (mixer_out, next_states, next_input, next_write, next_read)


def solution(mesh):
    return jax.shard_map(
        per_device,
        mesh=mesh,
        in_specs=(
            P(None, "kv"),
            P("kv"),
            P("kv", "tp"),
            P("kv", "tp"),
            P("kv", "tp"),
            P("kv", "tp"),
            P(),
            P(None, "tp"),
            P(None, "tp"),
            P(None, "tp"),
            P("tp"),
            P("tp"),
            P("tp"),
            P("kv", "tp"),
            P("tp"),
            P("tp", "kv"),
            P("kv", None, "tp", None, None),
            P("kv", None, "tp"),
            P("kv", None, "tp"),
            P("kv", None, "tp"),
            P("kv"),
        ),
        out_specs=(
            P("tp", "kv"),
            P("kv", None, "tp", None, None),
            P("kv", None, "tp"),
            P("kv", None, "tp"),
            P("kv", None, "tp"),
        ),
        check_vma=False,
    )
```

profile of v0, /device:TPU:1, one launch (start us, length us, event | category | flops | bytes accessed | tf_op | source)
XLA Modules:
  0.0 70.2 jit_solution(17013302515944873592)
XLA Ops:
  0.7 1.2 %fusion.5 = bf16[320]{0:T(512)(128)(2,1)S(1)} fusion(bf16[320,256]{1,0:T(8,128)(2,1)} %param.21), kind=kLoop, calls=%fused_computation.33 | loop fusion | flops 245440 | bytes 164480 | tf_op jit(solution)/shard_map/reduce_sum | solution.py:104
  1.9 1.1 %convolution_convert_fusion.6 = bf16[320,8]{0,1:T(8,128)(2,1)S(1)} fusion(bf16[320,256]{1,0:T(8,128)(2,1)} %param.21, f32[256]{0:T(256)} %param.22, bf16[4096,64]{0,1:T(8,128)(2,1)S(1)} %copy-done, s32[]{:T(128)S(6)} %select_n.14, s32[]{:T(128)S(6)} %select_n.15), kind=kOutput, calls=%fused_computation.8 | convolution fusion | flops 1559040 | bytes 174088 | tf_op jit(solution)/shard_map/dot_general | solution.py:110
  3.1 0.2 copy.85
  3.3 1.1 %convolution_convert_fusion.4 = bf16[320,128]{1,0:T(8,128)(2,1)S(1)} fusion(bf16[256,128]{1,0:T(8,128)(2,1)} %param.25, bf16[320,256]{1,0:T(8,128)(2,1)} %param.21, f32[256]{0:T(256)} %param.22), kind=kOutput, calls=%fused_computation.6 | convolution fusion | flops 21258240 | bytes 312320 | tf_op jit(solution)/shard_map/dot_general | solution.py:114
  4.5 1.1 %convolution_convert_fusion.3 = bf16[320,128]{1,0:T(8,128)(2,1)S(1)} fusion(bf16[256,128]{1,0:T(8,128)(2,1)} %param.26, bf16[320,256]{1,0:T(8,128)(2,1)} %param.21, f32[256]{0:T(256)} %param.22), kind=kOutput, calls=%fused_computation.5 | convolution fusion | flops 21258240 | bytes 312320 | tf_op jit(solution)/shard_map/dot_general | solution.py:114
  5.7 0.3 convert_element_type.115
  5.9 1.3 %convolution_convert_fusion.1 = bf16[320,512]{1,0:T(8,128)(2,1)S(1)} fusion(bf16[256,512]{1,0:T(8,128)(2,1)} %param.23, bf16[320,256]{1,0:T(8,128)(2,1)} %param.21, f32[256]{0:T(256)} %param.22), kind=kOutput, calls=%fused_computation.3 | convolution fusion | flops 84295680 | bytes 754688 | tf_op jit(solution)/shard_map/dot_general | solution.py:114
  7.3 1.3 %convolution_convert_fusion = bf16[320,512]{1,0:T(8,128)(2,1)S(1)} fusion(bf16[256,512]{1,0:T(8,128)(2,1)} %param.24, bf16[320,256]{1,0:T(8,128)(2,1)} %param.21, f32[256]{0:T(256)} %param.22), kind=kOutput, calls=%fused_computation.2 | convolution fusion | flops 84295680 | bytes 754688 | tf_op jit(solution)/shard_map/dot_general | solution.py:114
  8.7 1.7 %concatenate.32 = bf16[16,20,1289]{2,1,0:T(8,128)(2,1)} concatenate(bf16[16,20,512]{2,1,0:T(8,128)(2,1)S(1)} %concatenate.27, bf16[16,20,512]{2,1,0:T(8,128)(2,1)S(1)} %concatenate.28, bf16[16,20,128]{2,1,0:T(8,128)(2,1)S(1)} %concatenate.29, bf16[16,20,128]{2,1,0:T(8,128)(2,1)S(1)} %concatenate.30, bf16[16,20,8]{2,1,0:T(8,128)(2,1)S(1)} %copy.85, ...), dimensions={2} | concatenate | bytes 1649920 | tf_op jit(solution)/shard_map/concatenate | solution.py:34
  10.4 8.6 %all-to-all-start = ((bf16[16,20,1289]{2,1,0:T(8,128)(2,1)}), bf16[16,20,1289]{2,1,0:T(8,128)(2,1)S(1)}, u32[]{:S(2)}, u32[]{:S(2)}) async-start(bf16[16,20,1289]{2,1,0:T(8,128)(2,1)} %concatenate.32), calls=%async_computation | async-start | bytes 2162688 | tf_op jit(solution)/shard_map/all_to_all | solution.py:28
  19.1 0.2 convolution_convert_fusion.7
  19.3 0.2 convolution_convert_fusion.8
  19.5 0.2 convolution_convert_fusion.5
  20.0 3.8 %select_reduce_fusion = f32[4,8,64,128]{3,2,1,0:T(8,128)S(1)} fusion(f32[4,6,8,64,128]{4,3,2,1,0:T(8,128)} %param.37, pred[4,6]{1,0:T(4,128)(4,1)S(1)} %iota_compare_fusion.4), kind=kLoop, calls=%fused_computation | loop fusion | flops 2883584 | bytes 7340056 | tf_op jit(solution)/shard_map/reduce_sum | solution.py:167
  23.8 1.0 %bitcast_dynamic-update-slice_fusion = f32[4,6,8,64,128]{4,3,2,1,0:T(8,128)} fusion(f32[4,8,64,128]{3,2,1,0:T(8,128)S(1)} %select_reduce_fusion), kind=kLoop, calls=%fused_computation.11 | loop fusion | bytes 2097152
  24.8 10.6 %all-to-all-done = bf16[16,20,1289]{2,1,0:T(8,128)(2,1)S(1)} async-done(((bf16[16,20,1289]{2,1,0:T(8,128)(2,1)}), bf16[16,20,1289]{2,1,0:T(8,128)(2,1)S(1)}, u32[]{:S(2)}, u32[]{:S(2)}) %all-to-all-start) | async-done | bytes 824992 | tf_op jit(solution)/shard_map/all_to_all | solution.py:28
  35.6 0.2 fusion.21
  36.7 1.4 %multiply_reduce_fusion.3 = (f32[4,8,64]{2,1,0:T(8,128)S(1)}, f32[4,8,64]{2,1,0:T(8,128)S(1)}) fusion(f32[4,128]{1,0:T(4,128)S(1)} %bitcast.142, f32[4,128]{1,0:T(4,128)S(1)} %bitcast.124, f32[4,8,64]{2,1,0:T(8,128)S(1)} %get-tuple-element.15, f32[4,128]{1,0:T(4,128)S(1)} %bitcast.117, f32[4,8,64]{2,1,0:T(8,128)S(1)} %get-tuple-element.16, ...), kind=kLoop, calls=%fused_computation.23 | loop fusion | flops 2617344 | bytes 1089792 | tf_op jit(solution)/shard_map/reduce_sum | solution.py:178
  38.2 2.8 %multiply_reduce_fusion = (f32[4,8,64]{2,1,0:T(8,128)S(1)}, f32[4,8,64]{2,1,0:T(8,128)S(1)}, f32[4,8,64]{2,1,0:T(8,128)S(1)}) fusion(f32[4,128]{1,0:T(4,128)S(1)} %bitcast.140, f32[4,128]{1,0:T(4,128)S(1)} %bitcast.137, f32[4,8,64]{2,1,0:T(8,128)S(1)} %get-tuple-element.13, f32[4,8]{1,0:T(4,128)S(1)} %get-tuple-element.54, f32[4,128]{1,0:T(4,128)S(1)} %bitcast.134, ...), kind=kLoop, calls=%fused_computation.18 | loop fusion | flops 5498880 | bytes 1131136 | tf_op jit(solution)/shard_map/reduce_sum | solution.py:178
  41.6 0.8 %broadcast_in_dim.12 = bf16[16,20,512]{2,1,0:T(8,128)(2,1)} broadcast(bf16[20,512]{1,0:T(8,128)(2,1)S(1)} %multiply_convert_fusion), dimensions={1,2} | broadcast | bytes 348160 | tf_op jit(solution)/shard_map/broadcast_in_dim | solution.py:53
  42.4 4.7 %all-to-all-start.1 = ((bf16[16,20,512]{2,1,0:T(8,128)(2,1)}), bf16[16,20,512]{2,1,0:T(8,128)(2,1)S(1)}, u32[]{:S(2)}, u32[]{:S(2)}) async-start(bf16[16,20,512]{2,1,0:T(8,128)(2,1)} %broadcast_in_dim.12), calls=%async_computation.1 | async-start | bytes 786432 | tf_op jit(solution)/shard_map/all_to_all | solution.py:52
  47.1 1.4 %fusion.3 = f32[4,6,8,64,128]{4,3,2,1,0:T(8,128)} fusion(f32[4,6,8,64,128]{4,3,2,1,0:T(8,128)} %bitcast_dynamic-update-slice_fusion, f32[4,8,64,128]{3,2,1,0:T(8,128)S(1)} %select_reduce_fusion, f32[4,128]{1,0:T(4,128)S(1)} %bitcast.119, f32[4,8,64]{2,1,0:T(8,128)S(1)} %get-tuple-element.16, f32[4,8]{1,0:T(4,128)S(1)} %get-tuple-element.51), kind=kLoop, calls=%fused_computation.29 | loop fusion | flops 786432 | bytes 2107520
  48.5 1.6 %fusion.1 = f32[4,6,8,64,128]{4,3,2,1,0:T(8,128)} fusion(f32[4,6,8,64,128]{4,3,2,1,0:T(8,128)} %fusion.3, f32[4,8,64,128]{3,2,1,0:T(8,128)S(1)} %select_reduce_fusion, f32[4,128]{1,0:T(4,128)S(1)} %bitcast.126, f32[4,8,64]{2,1,0:T(8,128)S(1)} %get-tuple-element.15, f32[4,8]{1,0:T(4,128)S(1)} %get-tuple-element.52, f32[4,128]{1,0:T(4,128)S(1)} %bitcast.120, ...), kind=kLoop, calls=%fused_computation.27 | loop fusion | flops 1572864 | bytes 2117888
  50.0 1.9 %constant_dynamic-update-slice_fusion.5 = f32[4,6,8,64,128]{4,3,2,1,0:T(8,128)} fusion(f32[4,6,8,64,128]{4,3,2,1,0:T(8,128)} %fusion.1, f32[4,128]{1,0:T(4,128)S(1)} %bitcast.131, f32[4,8,64]{2,1,0:T(8,128)S(1)} %get-tuple-element.12, f32[4,128]{1,0:T(4,128)S(1)} %bitcast.127, f32[4,8,64]{2,1,0:T(8,128)S(1)} %get-tuple-element.15, ...), kind=kLoop, calls=%fused_computation.59 | loop fusion | flops 2359296 | bytes 2128256
  51.9 2.5 %fusion.2 = f32[4,6,8,64,128]{4,3,2,1,0:T(8,128)} fusion(f32[4,6,8,64,128]{4,3,2,1,0:T(8,128)} %constant_dynamic-update-slice_fusion.5, f32[4,128]{1,0:T(4,128)S(1)} %bitcast.135, f32[4,8,64]{2,1,0:T(8,128)S(1)} %get-tuple-element.14, f32[4,8]{1,0:T(4,128)S(1)} %get-tuple-element.53, f32[4,128]{1,0:T(4,128)S(1)} %bitcast.132, ...), kind=kLoop, calls=%fused_computation.28 | loop fusion | flops 3145728 | bytes 2138624
  54.5 2.8 %add_dynamic-update-slice_fusion = f32[4,6,8,64,128]{4,3,2,1,0:T(8,128)} fusion(f32[4,6,8,64,128]{4,3,2,1,0:T(8,128)} %fusion.2, f32[4,128]{1,0:T(4,128)S(1)} %bitcast.138, f32[4,8,64]{2,1,0:T(8,128)S(1)} %get-tuple-element.13, f32[4,8]{1,0:T(4,128)S(1)} %get-tuple-element.54, f32[4,128]{1,0:T(4,128)S(1)} %bitcast.136, ...), kind=kLoop, calls=%fused_computation.14 | loop fusion | flops 3932160 | bytes 2148992 | tf_op jit(solution)/shard_map/stack | solution.py:191
  57.3 0.9 %convolution_convert_fusion.2 = bf16[320,256]{1,0:T(8,128)(2,1)} fusion(bf16[320,512]{1,0:T(8,128)(2,1)S(1)} %reshape.335, bf16[512,256]{1,0:T(8,128)(2,1)S(1)} %copy-done.1), kind=kOutput, calls=%fused_computation.4 | convolution fusion | flops 83968000 | bytes 753664 | tf_op jit(solution)/shard_map/dot_general | solution.py:187
  58.2 5.8 %all-to-all-start.2 = ((bf16[8,40,256]{2,1,0:T(8,128)(2,1)}), bf16[8,40,256]{2,1,0:T(8,128)(2,1)S(1)}, u32[]{:S(2)}, u32[]{:S(2)}) async-start(bf16[8,40,256]{2,1,0:T(8,128)(2,1)} %bitcast.42), calls=%async_computation.2 | async-start | bytes 327680 | tf_op jit(solution)/shard_map/all_to_all | solution.py:28
  64.0 0.6 pad_maximum_fusion.1
  64.6 0.6 pad_maximum_fusion
  65.3 4.3 %all-to-all-done.2 = bf16[8,40,256]{2,1,0:T(8,128)(2,1)S(1)} async-done(((bf16[8,40,256]{2,1,0:T(8,128)(2,1)}), bf16[8,40,256]{2,1,0:T(8,128)(2,1)S(1)}, u32[]{:S(2)}, u32[]{:S(2)}) %all-to-all-start.2) | async-done | bytes 163872 | tf_op jit(solution)/shard_map/all_to_all | solution.py:28
  69.6 0.6 reduce_sum.117
  (75 shorter events, 2.5 us)
Async XLA Ops:
  0.6 1.3 %copy-start = (bf16[4096,64]{0,1:T(8,128)(2,1)S(1)}, bf16[4096,64]{0,1:T(8,128)(2,1)}, u32[]{:S(2)}) copy-start(bf16[4096,64]{0,1:T(8,128)(2,1)} %param.27) | copy-start | bytes 1572868
  0.7 18.3 %copy-start.9 = (s32[4]{0:T(128)S(1)}, s32[4]{0:T(128)}, u32[]{:S(2)}) copy-start(s32[4]{0:T(128)} %param.41) | copy-start | bytes 52
  0.7 18.4 %copy-start.6 = (f32[4,128]{1,0:T(4,128)S(1)}, f32[4,128]{1,0:T(4,128)}, u32[]{:S(2)}) copy-start(f32[4,128]{1,0:T(4,128)} %param.29) | copy-start | bytes 6148
  0.7 18.4 %copy-start.7 = (f32[4,128]{1,0:T(4,128)S(1)}, f32[4,128]{1,0:T(4,128)}, u32[]{:S(2)}) copy-start(f32[4,128]{1,0:T(4,128)} %param.30) | copy-start | bytes 6148
  0.7 18.4 %copy-start.11 = (bf16[4,8,128]{2,1,0:T(8,128)(2,1)S(1)}, bf16[4,8,128]{2,1,0:T(8,128)(2,1)}, u32[]{:S(2)}) copy-start(bf16[4,8,128]{2,1,0:T(8,128)(2,1)} %param.40) | copy-start | bytes 24580
  0.7 18.6 %copy-start.12 = (bf16[4,8,128]{2,1,0:T(8,128)(2,1)S(1)}, bf16[4,8,128]{2,1,0:T(8,128)(2,1)}, u32[]{:S(2)}) copy-start(bf16[4,8,128]{2,1,0:T(8,128)(2,1)} %param.39) | copy-start | bytes 24580
  0.7 18.8 %copy-start.3 = (f32[4,512]{1,0:T(4,128)S(1)}, f32[4,512]{1,0:T(4,128)}, u32[]{:S(2)}) copy-start(f32[4,512]{1,0:T(4,128)} %param.28) | copy-start | bytes 24580
  0.7 18.8 %copy-start.10 = (bf16[4,8,512]{2,1,0:T(8,128)(2,1)S(1)}, bf16[4,8,512]{2,1,0:T(8,128)(2,1)}, u32[]{:S(2)}) copy-start(bf16[4,8,512]{2,1,0:T(8,128)(2,1)} %param.38) | copy-start | bytes 98308
  0.7 19.1 %copy-start.13 = (f32[8]{0:T(128)S(1)}, f32[8]{0:T(128)}, u32[]{:S(2)}) copy-start(f32[8]{0:T(128)} %param.32) | copy-start | bytes 100
  0.7 19.1 %copy-start.4 = (f32[20,8]{0,1:T(8,128)S(1)}, f32[20,8]{0,1:T(8,128)}, u32[]{:S(2)}) copy-start(f32[20,8]{0,1:T(8,128)} %param.34) | copy-start | bytes 1924
  10.4 25.0 %all-to-all-start = ((bf16[16,20,1289]{2,1,0:T(8,128)(2,1)}), bf16[16,20,1289]{2,1,0:T(8,128)(2,1)S(1)}, u32[]{:S(2)}, u32[]{:S(2)}) async-start(bf16[16,20,1289]{2,1,0:T(8,128)(2,1)} %concatenate.32), calls=%async_computation | async-start | bytes 2162688 | tf_op jit(solution)/shard_map/all_to_all | solution.py:28
  19.0 17.5 %copy-start.8 = (f32[8]{0:T(128)S(1)}, f32[8]{0:T(128)}, u32[]{:S(2)}) copy-start(f32[8]{0:T(128)} %param.31) | copy-start | bytes 100
  20.0 18.1 %copy-start.2 = (f32[8]{0:T(128)S(1)}, f32[8]{0:T(128)}, u32[]{:S(2)}) copy-start(f32[8]{0:T(128)} %param.33) | copy-start | bytes 100
  20.0 21.6 %copy-start.5 = (f32[512]{0:T(512)S(1)}, f32[512]{0:T(512)}, u32[]{:S(2)}) copy-start(f32[512]{0:T(512)} %param.35) | copy-start | bytes 6148
  41.6 15.7 %copy-start.1 = (bf16[512,256]{1,0:T(8,128)(2,1)S(1)}, bf16[512,256]{1,0:T(8,128)(2,1)}, u32[]{:S(2)}) copy-start(bf16[512,256]{1,0:T(8,128)(2,1)} %param.36) | copy-start | bytes 786436
  42.4 14.8 %all-to-all-start.1 = ((bf16[16,20,512]{2,1,0:T(8,128)(2,1)}), bf16[16,20,512]{2,1,0:T(8,128)(2,1)S(1)}, u32[]{:S(2)}, u32[]{:S(2)}) async-start(bf16[16,20,512]{2,1,0:T(8,128)(2,1)} %broadcast_in_dim.12), calls=%async_computation.1 | async-start | bytes 786432 | tf_op jit(solution)/shard_map/all_to_all | solution.py:52
  58.2 11.3 %all-to-all-start.2 = ((bf16[8,40,256]{2,1,0:T(8,128)(2,1)}), bf16[8,40,256]{2,1,0:T(8,128)(2,1)S(1)}, u32[]{:S(2)}, u32[]{:S(2)}) async-start(bf16[8,40,256]{2,1,0:T(8,128)(2,1)} %bitcast.42), calls=%async_computation.2 | async-start | bytes 327680 | tf_op jit(solution)/shard_map/all_to_all | solution.py:28
where the time goes:
time: 70.7 us; the launch traced here: 70.2 us
  other arithmetic  22.6 us (32%)
  starting transfers between devices  19.1 us (27%)
  waiting for transfers between devices  14.9 us (21%)
  matrix products  7.41 us (10%)
  local copies, waits for them, and re-layouts  5.17 us (7%)
  between operations  1.04 us (1%)
    all_to_all x2, waiting for transfers between devices, sum_at_owner(): parts = lax.all_to_all(in_blocks(value, dim, peers), axis, 0, 0, tiled=True)  14.9 us
    all_to_all x2, starting transfers between devices, sum_at_owner(): parts = lax.all_to_all(in_blocks(value, dim, peers), axis, 0, 0, tiled=True)  14.4 us
    unnamed x8, other arithmetic  7.63 us
    dot_general x4, matrix products, per_device(): jnp.dot(scaled, weight, preferred_element_type=jnp.float32)  4.85 us
    all_to_all x1, starting transfers between devices, copy_for_each(): lax.all_to_all(jnp.broadcast_to(value[None], (peers, *value.shape)), axis...  4.7 us
    reduce_sum x2, other arithmetic, per_device(): jnp.sum(carried * conv_read[:, position][:, :, None, :], axis=-1)  4.25 us
    reduce_sum x1, other arithmetic, per_device(): jnp.sum(jnp.where(chosen[:, :, None, None, None], cached_state_history, 0...  3.76 us
    another operation x1, other arithmetic, per_device(): next_states = jnp.stack(states, axis=1)  2.79 us
  transfers between devices with their start and end apart: 3, of which 2 were waited for; matrix products, arithmetic and copies ran while one was open for 24% of the time, Pallas kernels for 0%

commit v1 on v0

v1 whole, which is shorter than its diff:
```python
import functools

import jax
import jax.numpy as jnp
from jax import lax
from jax.experimental import pallas as pl
from jax.experimental.pallas import tpu as pltpu
from jax.sharding import PartitionSpec as P

D = 4096
HEAD_TOTAL = 64
P_SIZE = 64
N = 128
G = 8
TAPS = 4
DRAFT_TOKENS = 5
KEPT = TAPS - 1
epsilon = 1e-05

F32 = jnp.float32
BF16 = jnp.bfloat16
HIGHEST = lax.Precision.HIGHEST
VMEM_SPEC = pl.BlockSpec(memory_space=pltpu.VMEM)
HBM_SPEC = pl.BlockSpec(memory_space=pltpu.HBM)

COLUMN_TILES = 10
MISC_ROW = 16 * COLUMN_TILES
HALF_ROW = MISC_ROW + 16
BLOCK_ROWS = HALF_ROW + 8 * (COLUMN_TILES // 2)
NORMED_HALF_ROW = 64
NORMED_ROWS = 80


def nt(a, b, precision=None):
    return lax.dot_general(a, b, (((1,), (1,)), ((), ())), precision=precision, preferred_element_type=F32)


def rows_of(shape, axis):
    return lax.broadcasted_iota(jnp.int32, shape, axis)


def by_head(scalars, lanes):
    value = jnp.zeros(lanes.shape, F32)
    for h in range(8):
        value = jnp.where(lanes // P_SIZE == h, scalars[h], value)
    return value


def project_kernel(
    tokens, gain, w_in, w_gate, w_write, w_read, step_t, accepted, history, bias, decay_logs, bypass,
    saved_input, saved_write, saved_read, k_in, k_write, k_read, extra_t, out_gain, w_out,
    out, carried, rows, pick, to_input, to_write, to_read, to_k_in, to_k_write, to_k_read, to_extra, to_gain, to_w_out,
    here, here_gain, m_in, m_gate, m_write, m_read, step_block, s_accepted, s_bias, s_decay, s_bypass, sems,
):
    kv, tp = lax.axis_index("kv"), lax.axis_index("tp")
    step_source = step_t.at[
        pl.ds(pl.multiple_of(tp * 8, 8), 8), pl.ds(pl.multiple_of(kv * 256, 256), 256)
    ]
    pairs = (
        (accepted, s_accepted),
        (tokens, here),
        (gain, here_gain),
        (w_in, m_in),
        (w_gate, m_gate),
        (w_write, m_write),
        (w_read, m_read),
        (step_source, step_block.at[pl.ds(0, 8)]),
        (bias, s_bias),
        (decay_logs, s_decay),
        (bypass, s_bypass),
        (saved_input, to_input),
        (saved_write, to_write),
        (saved_read, to_read),
        (k_in, to_k_in),
        (k_write, to_k_write),
        (k_read, to_k_read),
        (extra_t, to_extra),
        (out_gain, to_gain),
        (w_out, to_w_out),
    )
    copies = [pltpu.make_async_copy(a, b, sems.at[k]) for k, (a, b) in enumerate(pairs)]
    for copy in copies:
        copy.start()
    step_block[8:, :] = jnp.zeros((120, 256), BF16)
    row = rows_of((320, 320), 0)
    column = rows_of((320, 320), 1)
    source = jnp.where(
        row < 256, (row // 16) * 20 + row % 16, ((row - 256) // 4) * 20 + 16 + row % 4
    )
    order = jnp.where(column == source, 1.0, 0.0).astype(BF16)
    copies[0].wait()
    for s in range(4):
        fetch = pltpu.make_async_copy(history.at[s, s_accepted[s]], carried.at[s], sems.at[len(pairs) + s])
        fetch.start()
        copies.append(fetch)
    copies[1].wait()
    copies[2].wait()
    wide = jnp.dot(order, here[...], preferred_element_type=F32)
    squares = jnp.sum(wide * wide, axis=1, keepdims=True)
    scaled = (wide * here_gain[...]).astype(BF16)
    low = rows_of((8, 8, 128), 1) < 4

    def put(part, first):
        tiles = part.shape[1] // 128
        for k in range(tiles):
            tile = part[:256, 128 * k : 128 * k + 128].astype(BF16)
            spot = 16 * (first + k)
            out[:, :, spot : spot + 16, :] = tile.reshape(8, 2, 16, 128)
        for k in range(0, tiles, 2):
            one = part[256:, 128 * k : 128 * k + 128].reshape(8, 8, 128)
            two = part[256:, 128 * k + 128 : 128 * k + 256].reshape(8, 8, 128)
            spot = HALF_ROW + 4 * (first + k)
            out[:, 0, spot : spot + 8, :] = jnp.where(low, one, pltpu.roll(two, 4, 1)).astype(BF16)
            out[:, 1, spot : spot + 8, :] = jnp.where(low, pltpu.roll(one, 4, 1), two).astype(BF16)

    copies[3].wait()
    put(jnp.dot(scaled, m_in[...], preferred_element_type=F32), 0)
    copies[4].wait()
    put(jnp.dot(scaled, m_gate[...], preferred_element_type=F32), 4)
    copies[5].wait()
    copies[6].wait()
    put(
        jnp.concatenate(
            [
                jnp.dot(scaled, m_write[...], preferred_element_type=F32),
                jnp.dot(scaled, m_read[...], preferred_element_type=F32),
            ],
            axis=1,
        ),
        8,
    )
    copies[7].wait()
    misc = nt(scaled, step_block[...])
    misc = jnp.where(rows_of((320, 128), 1) == 8, squares, misc)
    full = misc[:256].reshape(8, 2, 16, 128)
    half = misc[256:].reshape(8, 8, 128)
    even = pltpu.roll(jnp.where(low, half, 0.0), 64, 2)
    odd = pltpu.roll(jnp.where(low, pltpu.roll(half, 4, 1), 0.0), 64, 2)
    out[:, 0, MISC_ROW : MISC_ROW + 16, :] = jnp.concatenate(
        [full[:, 0, :8] + even, full[:, 0, 8:]], axis=1
    ).astype(BF16)
    out[:, 1, MISC_ROW : MISC_ROW + 16, :] = jnp.concatenate(
        [full[:, 1, :8] + odd, full[:, 1, 8:]], axis=1
    ).astype(BF16)
    pick_row, pick_column = rows_of((32, 32), 0), rows_of((32, 32), 1)
    start = jnp.zeros((32, 32), jnp.int32)
    for s in range(4):
        start = jnp.where(pick_row // 8 == s, s_accepted[s] + 8 * s, start)
    pick[...] = jnp.where(
        (pick_row % 8 < KEPT) & (pick_column == start + pick_row % 8), 1.0, 0.0
    ).astype(BF16)
    for copy in copies[8:]:
        copy.wait()
    lanes = rows_of((8, 512), 1)
    rows[0] = by_head(s_bias, lanes)
    rows[1] = jnp.exp(by_head(s_decay, lanes))
    rows[2] = by_head(s_bypass, lanes)


def to_windows(first, second, half, half_high):
    row = rows_of(first.shape, 0)
    last = half if half_high else pltpu.roll(half, 4, 0)
    tiles = (
        pltpu.roll(first, 3, 0),
        jnp.where(row < 6, pltpu.roll(first, 6, 0), pltpu.roll(second, 6, 0)),
        pltpu.roll(second, 1, 0),
        jnp.where(row < 4, pltpu.roll(second, 4, 0), last),
    )
    return jnp.concatenate([jnp.where(row >= KEPT, t, 0.0) for t in tiles], axis=0)


def mix_kernel(
    received, carried, rows, pick, saved_input, saved_write, saved_read, k_in, k_write, k_read, extra_t, out_gain,
    copies, windows, step_x, keeps, writes,
):
    total = received[0].astype(F32)
    for k in range(1, 16):
        total = total + received[k].astype(F32)

    misc = total[MISC_ROW : MISC_ROW + 16]
    misc = to_windows(misc[:8], misc[8:], pltpu.roll(misc[:8], 64, 1), False)
    inverse = lax.rsqrt(misc[:, 8:9] / D + epsilon)

    def fresh(c):
        q = HALF_ROW + 8 * (c // 2)
        tile = to_windows(
            total[16 * c : 16 * c + 8], total[16 * c + 8 : 16 * c + 16], total[q : q + 8], c % 2 == 1
        )
        return (tile * inverse).astype(BF16)

    def joined(first, count):
        return jnp.concatenate([fresh(c) for c in range(first, first + count)], axis=1).astype(F32)

    def window(saved, first, count):
        flat = saved[...].reshape(32, 128 * count)
        return jnp.dot(pick[...], flat, preferred_element_type=F32) + joined(first, count)

    def convolve(value, taps):
        result = value * taps[KEPT : KEPT + 1, :]
        for k in range(KEPT):
            result = result + pltpu.roll(value, KEPT - k, 0) * taps[k : k + 1, :]
        return result * jax.nn.sigmoid(result)

    window_input = window(saved_input, 0, 4)
    window_write = window(saved_write, 8, 1)
    window_read = window(saved_read, 9, 1)
    gate = joined(4, 4)
    windows[:, :512] = window_input.astype(BF16)
    windows[:, 512:640] = window_write.astype(BF16)
    windows[:, 640:] = window_read.astype(BF16)
    conv_input = convolve(window_input, k_in)
    conv_write = convolve(window_write, k_write)
    conv_read = convolve(window_read, k_read)

    spread = jnp.where(
        rows_of((128, 512), 0) == rows_of((128, 512), 1) // P_SIZE, 1.0, 0.0
    )
    row8 = rows_of((32, 512), 0) % 8
    live = row8 >= KEPT
    step_raw = jnp.dot(misc, spread, precision=HIGHEST, preferred_element_type=F32) * inverse
    step = jnp.where(live, jax.nn.softplus(step_raw + rows[0, :1]), 0.0)
    token_row, token = rows_of((32, 20), 0), rows_of((32, 20), 1)
    place = jnp.where(
        (token_row % 8 >= KEPT) & (token == (token_row // 8) * 5 + token_row % 8 - KEPT), 1.0, 0.0
    )
    extra = jnp.dot(
        nt(place, extra_t[...], HIGHEST), spread[:8], precision=HIGHEST, preferred_element_type=F32
    )
    log_keep = jnp.where(live, extra - step * rows[1, :1], 0.0)
    total_log = log_keep + pltpu.roll(log_keep, 1, 0)
    total_log = jnp.where(live, total_log, 0.0)
    total_log = total_log + pltpu.roll(total_log, 2, 0)
    total_log = jnp.where(live, total_log, 0.0)
    total_log = total_log + jnp.where(row8 == 7, pltpu.roll(total_log, 4, 0), 0.0)
    scaled_x = step * conv_input
    step_x[...] = scaled_x
    keeps[...] = jnp.exp(log_keep)
    writes[...] = conv_write

    skip = rows[2, :1] * conv_input
    gate = gate * jax.nn.sigmoid(gate)
    tile_row = rows_of((8, 512), 0)
    normed = []
    for s in range(4):
        at = slice(8 * s, 8 * s + 8)
        logs, x, read = total_log[at], scaled_x[at], conv_read[at]
        weight = nt(read, conv_write[at], HIGHEST)
        value = skip[at]
        for i in range(KEPT, 8):
            keep = jnp.exp(jnp.minimum(logs - logs[i : i + 1], 0.0))
            term = weight[:, i : i + 1] * keep * x[i : i + 1]
            value = value + jnp.where(tile_row >= i, term, 0.0)
        state = carried[s].reshape(512, N).astype(BF16)
        value = value + jnp.exp(logs) * nt(read.astype(BF16), state)
        gated = value * gate[at]
        gated = gated * lax.rsqrt(jnp.mean(gated * gated, axis=1, keepdims=True) + epsilon)
        normed.append(gated * out_gain[...])

    first = jnp.where(tile_row < 5, pltpu.roll(normed[0], 5, 0), pltpu.roll(normed[1], 2, 0))
    last = pltpu.roll(normed[3], 4, 0)
    second = jnp.where(tile_row < 2, pltpu.roll(normed[1], 2, 0), pltpu.roll(normed[2], 7, 0))
    second = jnp.where(tile_row < 7, second, last)
    both = jnp.concatenate([first, second], axis=0).astype(BF16)
    block = [both[:, 128 * c : 128 * c + 128] for c in range(4)]
    for q in range(2):
        low = last[:, 256 * q : 256 * q + 128]
        high = normed[3][:, 256 * q + 128 : 256 * q + 256]
        block.append(jnp.where(tile_row[:, :128] < 4, low, high).astype(BF16))
    block = jnp.concatenate(block, axis=0)
    copies[...] = jnp.broadcast_to(block[None], copies.shape)


def state_kernel(
    carried, windows, step_x, keeps, writes, states, next_in, next_write, next_read,
    held, held_in, held_write, held_read, sems,
):
    copies = []

    def send(source, target):
        copy = pltpu.make_async_copy(source, target, sems.at[len(copies)])
        copy.start()
        copies.append(copy)

    for s in range(4):
        at = pl.ds(8 * s, 8)
        x = step_x[at, :].T
        for h in range(8):
            state = carried[s, h]
            held[s, 0, h] = state
            for r in range(KEPT, 8):
                keep = jnp.broadcast_to(
                    keeps[8 * s + r : 8 * s + r + 1, P_SIZE * h : P_SIZE * h + 1], (P_SIZE, N)
                )
                state = keep * state + x[P_SIZE * h : P_SIZE * h + P_SIZE, r : r + 1] * writes[8 * s + r : 8 * s + r + 1, :]
                held[s, r - KEPT + 1, h] = state
        held_in[s] = windows[at, :512]
        held_write[s] = windows[at, 512:640]
        held_read[s] = windows[at, 640:]
        send(held.at[s], states.at[s])
    send(held_in, next_in)
    send(held_write, next_write)
    send(held_read, next_read)
    for copy in copies:
        copy.wait()


def output_kernel(received, matrix, after, out):
    del after
    left = jnp.concatenate(
        [received[:, 16 * c : 16 * c + 16, :].reshape(256, 128) for c in range(4)], axis=1
    )
    full = jnp.dot(left, matrix[...], preferred_element_type=F32)
    halves = [
        received[:, NORMED_HALF_ROW + 8 * q : NORMED_HALF_ROW + 8 * q + 8, :].reshape(128, 128)
        for q in range(2)
    ]
    left = jnp.concatenate(halves, axis=1)
    low = jnp.dot(left, jnp.concatenate([matrix[0:128], matrix[256:384]], axis=0), preferred_element_type=F32)
    high = jnp.dot(left, jnp.concatenate([matrix[128:256], matrix[384:512]], axis=0), preferred_element_type=F32)
    half = low.reshape(16, 8, 256) + pltpu.roll(high.reshape(16, 8, 256), 4, 1)
    half = half.reshape(8, 2, 8, 256)
    tail = jnp.where(rows_of((8, 8, 256), 1) < 4, half[:, 0], pltpu.roll(half[:, 1], 4, 1))
    out[:, :32, :] = full.reshape(8, 32, 256).astype(BF16)
    out[:, 32:, :] = tail.astype(BF16)


def sum_kernel(received, out):
    total = received[0].astype(F32)
    for k in range(1, 8):
        total = total + received[k].astype(F32)
    low = rows_of((8, 256), 0) < 4
    third, fourth, half = pltpu.roll(total[16:24], 4, 0), pltpu.roll(total[24:32], 4, 0), total[32:]
    out[...] = jnp.concatenate(
        [
            total[:16],
            jnp.where(low, half, third),
            jnp.where(low, third, fourth),
            jnp.where(low, fourth, half),
        ],
        axis=0,
    ).astype(BF16)


def exchange(value, axis):
    return lax.all_to_all(value, axis, 0, 0, tiled=True)


def per_device(
    tokens,
    input_norm_gain,
    input_matrix,
    gate_matrix,
    write_matrix,
    read_matrix,
    step_matrix,
    input_kernel,
    write_kernel,
    read_kernel,
    step_size_bias,
    head_decay_logs,
    bypass_scale,
    extra_decay_logs,
    output_norm_gain,
    output_matrix,
    cached_state_history,
    cached_input_rows,
    cached_write_rows,
    cached_read_rows,
    accepted,
):
    bf16_of = functools.partial(jax.ShapeDtypeStruct, dtype=BF16)
    f32_of = functools.partial(jax.ShapeDtypeStruct, dtype=F32)
    sent, carried, rows, pick, *kept, matrix = pl.pallas_call(
        project_kernel,
        out_shape=(
            bf16_of((8, 2, BLOCK_ROWS, 128)),
            f32_of((4, 8, P_SIZE, N)),
            f32_of((3, 8, 512)),
            bf16_of((32, 32)),
            bf16_of((4, 8, 512)),
            bf16_of((4, 8, N)),
            bf16_of((4, 8, N)),
            f32_of((TAPS, 512)),
            f32_of((TAPS, N)),
            f32_of((TAPS, N)),
            f32_of((8, 20)),
            f32_of((1, 512)),
            bf16_of((512, 256)),
        ),
        in_specs=[HBM_SPEC] * 21,
        out_specs=(VMEM_SPEC,) * 13,
        scratch_shapes=[
            pltpu.VMEM((320, 256), BF16),
            pltpu.VMEM((1, 256), F32),
            pltpu.VMEM((256, 512), BF16),
            pltpu.VMEM((256, 512), BF16),
            pltpu.VMEM((256, 128), BF16),
            pltpu.VMEM((256, 128), BF16),
            pltpu.VMEM((128, 256), BF16),
            pltpu.SMEM((4,), jnp.int32),
            pltpu.SMEM((8,), F32),
            pltpu.SMEM((8,), F32),
            pltpu.SMEM((8,), F32),
            pltpu.SemaphoreType.DMA((24,)),
        ],
        compiler_params=pltpu.CompilerParams(vmem_limit_bytes=16 << 20),
        name="project",
    )(
        *(pltpu.with_memory_space_constraint(a, pltpu.HBM) for a in (
        tokens,
        input_norm_gain.reshape(1, 256),
        input_matrix,
        gate_matrix,
        write_matrix,
        read_matrix,
        step_matrix.T,
        accepted,
        cached_state_history,
        step_size_bias,
        head_decay_logs,
        bypass_scale,
        cached_input_rows,
        cached_write_rows,
        cached_read_rows,
        input_kernel,
        write_kernel,
        read_kernel,
        extra_decay_logs.T,
        output_norm_gain.reshape(1, 512),
        output_matrix,
        ))
    )
    received = exchange(sent.reshape(16, BLOCK_ROWS, 128), "kv")
    copies, windows, step_x, keeps, writes = pl.pallas_call(
        mix_kernel,
        out_shape=(
            bf16_of((16, NORMED_ROWS, 128)),
            bf16_of((32, 768)),
            f32_of((32, 512)),
            f32_of((32, 512)),
            f32_of((32, N)),
        ),
        in_specs=[VMEM_SPEC] * 12,
        out_specs=(VMEM_SPEC,) * 5,
        compiler_params=pltpu.CompilerParams(vmem_limit_bytes=16 << 20),
        name="mix",
    )(received, carried, rows, pick, *kept)
    everyone = exchange(copies, "kv")
    next_states, next_input, next_write, next_read = pl.pallas_call(
        state_kernel,
        out_shape=(
            f32_of((4, 6, 8, P_SIZE, N)),
            bf16_of((4, 8, 512)),
            bf16_of((4, 8, N)),
            bf16_of((4, 8, N)),
        ),
        in_specs=[VMEM_SPEC] * 5,
        out_specs=(HBM_SPEC,) * 4,
        scratch_shapes=[
            pltpu.VMEM((4, 6, 8, P_SIZE, N), F32),
            pltpu.VMEM((4, 8, 512), BF16),
            pltpu.VMEM((4, 8, N), BF16),
            pltpu.VMEM((4, 8, N), BF16),
            pltpu.SemaphoreType.DMA((7,)),
        ],
        compiler_params=pltpu.CompilerParams(vmem_limit_bytes=16 << 20),
        cost_estimate=pl.CostEstimate(flops=200_000_000, bytes_accessed=8_000_000, transcendentals=0),
        name="states",
    )(carried, windows, step_x, keeps, writes)
    partial_sums = pl.pallas_call(
        output_kernel,
        out_shape=jax.ShapeDtypeStruct((8, 40, 256), BF16),
        in_specs=[VMEM_SPEC] * 2 + [HBM_SPEC],
        out_specs=VMEM_SPEC,
        compiler_params=pltpu.CompilerParams(vmem_limit_bytes=8 << 20),
        name="output",
    )(everyone, matrix, pltpu.with_memory_space_constraint(next_write, pltpu.HBM))
    mixer_out = pl.pallas_call(
        sum_kernel,
        out_shape=jax.ShapeDtypeStruct((40, 256), BF16),
        in_specs=[VMEM_SPEC],
        out_specs=VMEM_SPEC,
        compiler_params=pltpu.CompilerParams(vmem_limit_bytes=4 << 20),
        name="total",
    )(exchange(partial_sums, "tp"))
    return (mixer_out, next_states, next_input, next_write, next_read)


def solution(mesh):
    return jax.shard_map(
        per_device,
        mesh=mesh,
        in_specs=(
            P(None, "kv"),
            P("kv"),
            P("kv", "tp"),
            P("kv", "tp"),
            P("kv", "tp"),
            P("kv", "tp"),
            P(),
            P(None, "tp"),
            P(None, "tp"),
            P(None, "tp"),
            P("tp"),
            P("tp"),
            P("tp"),
            P("kv", "tp"),
            P("tp"),
            P("tp", "kv"),
            P("kv", None, "tp", None, None),
            P("kv", None, "tp"),
            P("kv", None, "tp"),
            P("kv", None, "tp"),
            P("kv"),
        ),
        out_specs=(
            P("tp", "kv"),
            P("kv", None, "tp", None, None),
            P("kv", None, "tp"),
            P("kv", None, "tp"),
            P("kv", None, "tp"),
        ),
        check_vma=False,
    )
```

time: 70.7 us -> 53.1 us (0.75)
  blocking collectives: 0 us -> 35.5 us
  other arithmetic: 22.6 us -> 0 us
  starting transfers between devices: 19.1 us -> 3.54 us
  waiting for transfers between devices: 14.9 us -> 3.57 us
  Pallas kernels: 0 us -> 9.58 us
  matrix products: 7.41 us -> 0 us
  local copies, waits for them, and re-layouts: 5.17 us -> 0 us
    all_to_all x0 -> x2, blocking collectives: none -> 35.5 us  [exchange(): return lax.all_to_all(value, axis, 0, 0, tiled=True)]
    all_to_all x3 -> x1, starting transfers between devices: 19.1 us -> 3.54 us  [exchange(): return lax.all_to_all(value, axis, 0, 0, tiled=True)]
    all_to_all x3 -> x1, waiting for transfers between devices: 14.9 us -> 3.57 us  [exchange(): return lax.all_to_all(value, axis, 0, 0, tiled=True)]
    reduce_sum x7 -> x0, other arithmetic: 10.1 us -> none  [the longest x2 4.25 us: per_device(): jnp.sum(carried * conv_read[:, position][:, :, None, :], axis=-1)]
    pallas_call x0 -> x5, Pallas kernels: none -> 9.58 us  [the longest x1 4.35 us: per_device(): pl.pallas_call(state_kernel, out_shape=(f32_of((4, 6, 8, P_SIZE, N)), bf1...]
    unnamed x8 -> x0, other arithmetic: 7.63 us -> none
    dot_general x9 -> x0, matrix products: 7.41 us -> none  [the longest x4 4.85 us: per_device(): jnp.dot(scaled, weight, preferred_element_type=jnp.float32)]
    another operation x2 -> x0, other arithmetic: 2.86 us -> none  [the longest x1 2.79 us: per_device(): next_states = jnp.stack(states, axis=1)]
  transfers between devices with their start and end apart: 3 -> 1, of which waited for: 2 -> 1; matrix products, arithmetic and copies ran while one was open for 24% -> 0% of each run, Pallas kernels for 0% -> 8%
where the time goes in v1:
time: 53.1 us; the launch traced here: 52.8 us
  blocking collectives  35.5 us (67%)
  Pallas kernels  9.58 us (18%)
  waiting for transfers between devices  3.57 us (7%)
  starting transfers between devices  3.54 us (7%)
  between operations  0.67 us (1%)
    all_to_all x2, blocking collectives, exchange(): return lax.all_to_all(value, axis, 0, 0, tiled=True)  35.5 us
    pallas_call x1, Pallas kernels, per_device(): pl.pallas_call(state_kernel, out_shape=(f32_of((4, 6, 8, P_SIZE, N)), bf1...  4.35 us
    all_to_all x1, waiting for transfers between devices, exchange(): return lax.all_to_all(value, axis, 0, 0, tiled=True)  3.57 us
    all_to_all x1, starting transfers between devices, exchange(): return lax.all_to_all(value, axis, 0, 0, tiled=True)  3.54 us
    pallas_call x1, Pallas kernels, per_device(): pl.pallas_call(project_kernel, out_shape=(bf16_of((8, 2, BLOCK_ROWS, 128)...  2.7 us
    pallas_call x1, Pallas kernels, per_device(): pl.pallas_call(mix_kernel, out_shape=(bf16_of((16, NORMED_ROWS, 128)), bf...  1.62 us
  transfers between devices with their start and end apart: 1, of which 1 were waited for; matrix products, arithmetic and copies ran while one was open for 0% of the time, Pallas kernels for 8%

profile of v1, /device:TPU:1, one launch (start us, length us, event | category | flops | bytes accessed | tf_op | source)
XLA Modules:
  0.0 52.8 jit_solution(2210875295364489538)
XLA Ops:
  0.6 2.7 %project.1 = (bf16[8,2,216,128]{3,2,1,0:T(8,128)(2,1)S(1)}, f32[4,8,64,128]{3,2,1,0:T(8,128)S(1)}, f32[3,8,512]{2,1,0:T(8,128)S(1)}, bf16[32,32]{1,0:T(8,128)(2,...) custom-call(bf16[320,256]{1,0:T(8,128)(2,1)} %tokens.1, ...), custom_call_target="tpu_custom_call" | custom-call | tf_op jit(solution)/shard_map/project/pallas_call | solution.py:373
  3.4 22.9 %all_to_all.15.received = bf16[16,216,128]{2,1,0:T(8,128)(2,1)S(1)} all-to-all(bf16[16,216,128]{2,1,0:T(8,128)(2,1)S(1)} %bitcast.5), channel_id=1, replica_groups=mesh['kv'=16,'tp'=8] {'kv'}, dimensions={0} | all-to-all | bytes 1769472 | tf_op jit(solution)/shard_map/all_to_all | solution.py:345
  26.3 1.6 %mix.1 = (bf16[16,80,128]{2,1,0:T(8,128)(2,1)}, bf16[32,768]{1,0:T(8,128)(2,1)S(1)}, f32[32,512]{1,0:T(8,128)S(1)}, f32[32,512]{1,0:T(8,128)S(1)}, f32[32,128]{1,0:T(8,128)S(1)}) custom-call(bf16[16,216,128]{2,1,0:T(8,128)(2,1)S(1)} %all_to_all.15.received, f32[4,8,64,128]{3,2,1,0:T(8,128)S(1)} %get-tuple-element.28.carried, ...), custom_call_target="tpu_custom_call" | custom-call | tf_op jit(solution)/shard_map/mix/pallas_call | solution.py:434
  27.9 3.5 %all-to-all-start.1 = ((bf16[16,80,128]{2,1,0:T(8,128)(2,1)}), bf16[16,80,128]{2,1,0:T(8,128)(2,1)S(1)}, u32[]{:S(2)}, u32[]{:S(2)}) async-start(bf16[16,80,128]{2,1,0:T(8,128)(2,1)} %get-tuple-element.39), calls=%async_computation.1 | async-start | bytes 655360 | tf_op jit(solution)/shard_map/all_to_all | solution.py:345
  31.5 4.3 %states.1 = (f32[4,6,8,64,128]{4,3,2,1,0:T(8,128)}, bf16[4,8,512]{2,1,0:T(8,128)(2,1)}, bf16[4,8,128]{2,1,0:T(8,128)(2,1)}, bf16[4,8,128]{2,1,0:T(8,128)(2,1)}) custom-call(f32[4,8,64,128]{3,2,1,0:T(8,128)S(1)} %get-tuple-element.28.carried, bf16[32,768]{1,0:T(8,128)(2,1)S(1)} %get-tuple-element.41.windows, f32[32,512]{1,0:T(8,128)S(1)} %get-tuple-element.42.step_x, ...), custom_call_target="tpu_custom_call" | custom-call | flops 200000000 | bytes 8000000 | tf_op jit(solution)/shard_map/states/pallas_call | solution.py:449
  35.8 3.6 %all-to-all-done.1.received = bf16[16,80,128]{2,1,0:T(8,128)(2,1)S(1)} async-done(((bf16[16,80,128]{2,1,0:T(8,128)(2,1)}), bf16[16,80,128]{2,1,0:T(8,128)(2,1)S(1)}, u32[]{:S(2)}, u32[]{:S(2)}) %all-to-all-start.1) | async-done | bytes 327712 | tf_op jit(solution)/shard_map/all_to_all | solution.py:345
  39.4 0.3 output.1
  39.7 12.5 %all_to_all.16.received = bf16[8,40,256]{2,1,0:T(8,128)(2,1)S(1)} all-to-all(bf16[8,40,256]{2,1,0:T(8,128)(2,1)S(1)} %output.1), channel_id=1, replica_groups=mesh['kv'=16,'tp'=8] {'tp'}, dimensions={0} | all-to-all | bytes 327680 | tf_op jit(solution)/shard_map/all_to_all | solution.py:345
  52.2 0.6 %total.1 = bf16[40,256]{1,0:T(8,128)(2,1)} custom-call(bf16[8,40,256]{2,1,0:T(8,128)(2,1)S(1)} %all_to_all.16.received), custom_call_target="tpu_custom_call" | custom-call | tf_op jit(solution)/shard_map/total/pallas_call | solution.py:478
Async XLA Ops:
  27.9 11.5 %all-to-all-start.1 = ((bf16[16,80,128]{2,1,0:T(8,128)(2,1)}), bf16[16,80,128]{2,1,0:T(8,128)(2,1)S(1)}, u32[]{:S(2)}, u32[]{:S(2)}) async-start(bf16[16,80,128]{2,1,0:T(8,128)(2,1)} %get-tuple-element.39), calls=%async_computation.1 | async-start | bytes 655360 | tf_op jit(solution)/shard_map/all_to_all | solution.py:345

commit v2 on v1

--- a/solution.py
+++ b/solution.py
@@ -25,7 +25,7 @@
 
 COLUMN_TILES = 10
 MISC_ROW = 16 * COLUMN_TILES
-HALF_ROW = MISC_ROW + 16
+HALF_ROW = MISC_ROW + 8
 BLOCK_ROWS = HALF_ROW + 8 * (COLUMN_TILES // 2)
 NORMED_HALF_ROW = 64
 NORMED_ROWS = 80
@@ -82,12 +82,6 @@
     for copy in copies:
         copy.start()
     step_block[8:, :] = jnp.zeros((120, 256), BF16)
-    row = rows_of((320, 320), 0)
-    column = rows_of((320, 320), 1)
-    source = jnp.where(
-        row < 256, (row // 16) * 20 + row % 16, ((row - 256) // 4) * 20 + 16 + row % 4
-    )
-    order = jnp.where(column == source, 1.0, 0.0).astype(BF16)
     copies[0].wait()
     for s in range(4):
         fetch = pltpu.make_async_copy(history.at[s, s_accepted[s]], carried.at[s], sems.at[len(pairs) + s])
@@ -95,23 +89,27 @@
         copies.append(fetch)
     copies[1].wait()
     copies[2].wait()
-    wide = jnp.dot(order, here[...], preferred_element_type=F32)
+    wide = here[...].astype(F32)
     squares = jnp.sum(wide * wide, axis=1, keepdims=True)
     scaled = (wide * here_gain[...]).astype(BF16)
     low = rows_of((8, 8, 128), 1) < 4
 
+    def tiles_of(part):
+        a, b, c, d, e = (part.reshape(8, 5, 8, 128)[:, k] for k in range(5))
+        middle, last = pltpu.roll(d, 4, 1), pltpu.roll(e, 4, 1)
+        turned = pltpu.roll(c, 4, 1)
+        return (a, b, c, turned), (jnp.where(low, turned, middle), jnp.where(low, middle, last), last, e)
+
     def put(part, first):
-        tiles = part.shape[1] // 128
-        for k in range(tiles):
-            tile = part[:256, 128 * k : 128 * k + 128].astype(BF16)
-            spot = 16 * (first + k)
-            out[:, :, spot : spot + 16, :] = tile.reshape(8, 2, 16, 128)
-        for k in range(0, tiles, 2):
-            one = part[256:, 128 * k : 128 * k + 128].reshape(8, 8, 128)
-            two = part[256:, 128 * k + 128 : 128 * k + 256].reshape(8, 8, 128)
-            spot = HALF_ROW + 4 * (first + k)
-            out[:, 0, spot : spot + 8, :] = jnp.where(low, one, pltpu.roll(two, 4, 1)).astype(BF16)
-            out[:, 1, spot : spot + 8, :] = jnp.where(low, pltpu.roll(one, 4, 1), two).astype(BF16)
+        sets = [tiles_of(part[:, 128 * k : 128 * k + 128]) for k in range(part.shape[1] // 128)]
+        for odd in range(2):
+            for k, both in enumerate(sets):
+                spot = 16 * (first + k)
+                out[:, odd, spot : spot + 16, :] = jnp.concatenate(both[odd][:2], axis=1).astype(BF16)
+            for k in range(0, len(sets), 2):
+                spot = HALF_ROW + 4 * (first + k)
+                half = jnp.where(low, sets[k][odd][2], sets[k + 1][odd][3])
+                out[:, odd, spot : spot + 8, :] = half.astype(BF16)
 
     copies[3].wait()
     put(jnp.dot(scaled, m_in[...], preferred_element_type=F32), 0)
@@ -132,16 +130,9 @@
     copies[7].wait()
     misc = nt(scaled, step_block[...])
     misc = jnp.where(rows_of((320, 128), 1) == 8, squares, misc)
-    full = misc[:256].reshape(8, 2, 16, 128)
-    half = misc[256:].reshape(8, 8, 128)
-    even = pltpu.roll(jnp.where(low, half, 0.0), 64, 2)
-    odd = pltpu.roll(jnp.where(low, pltpu.roll(half, 4, 1), 0.0), 64, 2)
-    out[:, 0, MISC_ROW : MISC_ROW + 16, :] = jnp.concatenate(
-        [full[:, 0, :8] + even, full[:, 0, 8:]], axis=1
-    ).astype(BF16)
-    out[:, 1, MISC_ROW : MISC_ROW + 16, :] = jnp.concatenate(
-        [full[:, 1, :8] + odd, full[:, 1, 8:]], axis=1
-    ).astype(BF16)
+    for odd, (one, two, half, _) in enumerate(tiles_of(jnp.where(rows_of((320, 128), 1) < 9, misc, 0.0))):
+        value = one + pltpu.roll(two, 32, 2) + jnp.where(low, pltpu.roll(half, 64, 2), 0.0)
+        out[:, odd, MISC_ROW : MISC_ROW + 8, :] = value.astype(BF16)
     pick_row, pick_column = rows_of((32, 32), 0), rows_of((32, 32), 1)
     start = jnp.zeros((32, 32), jnp.int32)
     for s in range(4):
@@ -177,8 +168,8 @@
     for k in range(1, 16):
         total = total + received[k].astype(F32)
 
-    misc = total[MISC_ROW : MISC_ROW + 16]
-    misc = to_windows(misc[:8], misc[8:], pltpu.roll(misc[:8], 64, 1), False)
+    misc = total[MISC_ROW : MISC_ROW + 8]
+    misc = to_windows(misc, pltpu.roll(misc, 96, 1), pltpu.roll(misc, 64, 1), False)
     inverse = lax.rsqrt(misc[:, 8:9] / D + epsilon)
 
     def fresh(c):
@@ -270,6 +261,11 @@
     copies[...] = jnp.broadcast_to(block[None], copies.shape)
 
 
+def in_pieces(value):
+    first = value.astype(BF16).astype(F32)
+    return first, value - first
+
+
 def state_kernel(
     carried, windows, step_x, keeps, writes, states, next_in, next_write, next_read,
     held, held_in, held_write, held_read, sems,
@@ -282,21 +278,31 @@
         copies.append(copy)
 
     for s in range(4):
+        send(carried.at[s], states.at[s, 0])
+    row, column = rows_of((8, DRAFT_TOKENS * N), 0), rows_of((8, DRAFT_TOKENS * N), 1)
+    own = row == column // N + KEPT
+    for s in range(4):
         at = pl.ds(8 * s, 8)
-        x = step_x[at, :].T
+        x_high, x_low = in_pieces(step_x[at, :])
+        w_high, w_low = (
+            jnp.where(own, jnp.concatenate([w] * DRAFT_TOKENS, axis=1), 0.0) for w in in_pieces(writes[at, :])
+        )
+        left = jnp.concatenate([x_high, x_high, x_low], axis=0).T.astype(BF16)
+        right = jnp.concatenate([w_high, w_low, w_high], axis=0).astype(BF16)
+        added = jnp.dot(left, right, preferred_element_type=F32)
         for h in range(8):
             state = carried[s, h]
-            held[s, 0, h] = state
-            for r in range(KEPT, 8):
-                keep = jnp.broadcast_to(
-                    keeps[8 * s + r : 8 * s + r + 1, P_SIZE * h : P_SIZE * h + 1], (P_SIZE, N)
-                )
-                state = keep * state + x[P_SIZE * h : P_SIZE * h + P_SIZE, r : r + 1] * writes[8 * s + r : 8 * s + r + 1, :]
-                held[s, r - KEPT + 1, h] = state
+            for r in range(DRAFT_TOKENS):
+                spot = 8 * s + KEPT + r
+                keep = jnp.broadcast_to(keeps[spot : spot + 1, P_SIZE * h : P_SIZE * h + 1], (P_SIZE, N))
+                state = keep * state + added[P_SIZE * h : P_SIZE * h + P_SIZE, N * r : N * r + N]
+                held[s, r, h] = state
+        send(held.at[s], states.at[s, pl.ds(1, DRAFT_TOKENS)])
+    for s in range(4):
+        at = pl.ds(8 * s, 8)
         held_in[s] = windows[at, :512]
         held_write[s] = windows[at, 512:640]
         held_read[s] = windows[at, 640:]
-        send(held.at[s], states.at[s])
     send(held_in, next_in)
     send(held_write, next_write)
     send(held_read, next_read)
@@ -304,8 +310,7 @@
         copy.wait()
 
 
-def output_kernel(received, matrix, after, out):
-    del after
+def output_kernel(received, matrix, out):
     left = jnp.concatenate(
         [received[:, 16 * c : 16 * c + 16, :].reshape(256, 128) for c in range(4)], axis=1
     )
@@ -457,11 +462,11 @@
         in_specs=[VMEM_SPEC] * 5,
         out_specs=(HBM_SPEC,) * 4,
         scratch_shapes=[
-            pltpu.VMEM((4, 6, 8, P_SIZE, N), F32),
+            pltpu.VMEM((4, DRAFT_TOKENS, 8, P_SIZE, N), F32),
             pltpu.VMEM((4, 8, 512), BF16),
             pltpu.VMEM((4, 8, N), BF16),
             pltpu.VMEM((4, 8, N), BF16),
-            pltpu.SemaphoreType.DMA((7,)),
+            pltpu.SemaphoreType.DMA((11,)),
         ],
         compiler_params=pltpu.CompilerParams(vmem_limit_bytes=16 << 20),
         cost_estimate=pl.CostEstimate(flops=200_000_000, bytes_accessed=8_000_000, transcendentals=0),
@@ -470,11 +475,11 @@
     partial_sums = pl.pallas_call(
         output_kernel,
         out_shape=jax.ShapeDtypeStruct((8, 40, 256), BF16),
-        in_specs=[VMEM_SPEC] * 2 + [HBM_SPEC],
+        in_specs=[VMEM_SPEC] * 2,
         out_specs=VMEM_SPEC,
         compiler_params=pltpu.CompilerParams(vmem_limit_bytes=8 << 20),
         name="output",
-    )(everyone, matrix, pltpu.with_memory_space_constraint(next_write, pltpu.HBM))
+    )(everyone, matrix)
     mixer_out = pl.pallas_call(
         sum_kernel,
         out_shape=jax.ShapeDtypeStruct((40, 256), BF16),

time: 53.1 us -> 52 us (0.979)
  starting transfers between devices: 3.54 us -> 6.83 us
  blocking collectives: 35.5 us -> 33.7 us
  Pallas kernels: 9.58 us -> 7.93 us
  waiting for transfers between devices: 3.57 us -> 2.57 us
    all_to_all x1, starting transfers between devices: 3.54 us -> 6.83 us  [exchange(): return lax.all_to_all(value, axis, 0, 0, tiled=True)]
    all_to_all x2, blocking collectives: 35.5 us -> 33.7 us  [exchange(): return lax.all_to_all(value, axis, 0, 0, tiled=True)]
    pallas_call x1, Pallas kernels: 4.35 us -> 2.97 us  [per_device(): pl.pallas_call(state_kernel, out_shape=(f32_of((4, 6, 8, P_SIZE, N)), bf1...]
    all_to_all x1, waiting for transfers between devices: 3.57 us -> 2.57 us  [exchange(): return lax.all_to_all(value, axis, 0, 0, tiled=True)]
    pallas_call x1, Pallas kernels: 1.62 us -> 0.93 us  [per_device(): pl.pallas_call(mix_kernel, out_shape=(bf16_of((16, NORMED_ROWS, 128)), bf...]
    pallas_call x1, Pallas kernels: 0.27 us -> 0.94 us  [per_device(): pl.pallas_call(output_kernel, out_shape=jax.ShapeDtypeStruct((8, 40, 256)...]
  transfers between devices with their start and end apart: 1 -> 1, of which waited for: 1 -> 1; matrix products, arithmetic and copies ran while one was open for 0% -> 0% of each run, Pallas kernels for 8% -> 6%
where the time goes in v2:
time: 52 us; the launch traced here: 51.7 us
  blocking collectives  33.7 us (65%)
  Pallas kernels  7.93 us (15%)
  starting transfers between devices  6.83 us (13%)
  waiting for transfers between devices  2.57 us (5%)
  between operations  0.67 us (1%)
    all_to_all x2, blocking collectives, exchange(): return lax.all_to_all(value, axis, 0, 0, tiled=True)  33.7 us
    all_to_all x1, starting transfers between devices, exchange(): return lax.all_to_all(value, axis, 0, 0, tiled=True)  6.83 us
    pallas_call x1, Pallas kernels, per_device(): pl.pallas_call(state_kernel, out_shape=(f32_of((4, 6, 8, P_SIZE, N)), bf1...  2.97 us
    all_to_all x1, waiting for transfers between devices, exchange(): return lax.all_to_all(value, axis, 0, 0, tiled=True)  2.57 us
    pallas_call x1, Pallas kernels, per_device(): pl.pallas_call(project_kernel, out_shape=(bf16_of((8, 2, BLOCK_ROWS, 128)...  2.46 us
  transfers between devices with their start and end apart: 1, of which 1 were waited for; matrix products, arithmetic and copies ran while one was open for 0% of the time, Pallas kernels for 6%

profile of v2, /device:TPU:1, one launch (start us, length us, event | category | flops | bytes accessed | tf_op | source)
XLA Modules:
  0.0 51.7 jit_solution(2283185873818959510)
XLA Ops:
  0.6 2.5 %project.1 = (bf16[8,2,208,128]{3,2,1,0:T(8,128)(2,1)S(1)}, f32[4,8,64,128]{3,2,1,0:T(8,128)S(1)}, f32[3,8,512]{2,1,0:T(8,128)S(1)}, bf16[32,32]{1,0:T(8,128)(2,...) custom-call(bf16[320,256]{1,0:T(8,128)(2,1)} %tokens.1, ...), custom_call_target="tpu_custom_call" | custom-call | tf_op jit(solution)/shard_map/project/pallas_call | solution.py:378
  3.1 22.6 %all_to_all.15.received = bf16[16,208,128]{2,1,0:T(8,128)(2,1)S(1)} all-to-all(bf16[16,208,128]{2,1,0:T(8,128)(2,1)S(1)} %bitcast.5), channel_id=1, replica_groups=mesh['kv'=16,'tp'=8] {'kv'}, dimensions={0} | all-to-all | bytes 1703936 | tf_op jit(solution)/shard_map/all_to_all | solution.py:350
  25.7 0.9 %mix.1 = (bf16[16,80,128]{2,1,0:T(8,128)(2,1)S(1)}, bf16[32,768]{1,0:T(8,128)(2,1)S(1)}, f32[32,512]{1,0:T(8,128)S(1)}, f32[32,512]{1,0:T(8,128)S(1)}, f32[32,128]{1,0:T(8,128)S(1)}) custom-call(bf16[16,208,128]{2,1,0:T(8,128)(2,1)S(1)} %all_to_all.15.received, f32[4,8,64,128]{3,2,1,0:T(8,128)S(1)} %get-tuple-element.28.carried, ...), custom_call_target="tpu_custom_call" | custom-call | tf_op jit(solution)/shard_map/mix/pallas_call | solution.py:439
  26.6 11.1 %all_to_all.16.received = bf16[16,80,128]{2,1,0:T(8,128)(2,1)S(1)} all-to-all(bf16[16,80,128]{2,1,0:T(8,128)(2,1)S(1)} %get-tuple-element.39), channel_id=1, replica_groups=mesh['kv'=16,'tp'=8] {'kv'}, dimensions={0} | all-to-all | bytes 655360 | tf_op jit(solution)/shard_map/all_to_all | solution.py:350
  37.8 0.9 %output.1 = bf16[8,40,256]{2,1,0:T(8,128)(2,1)} custom-call(bf16[16,80,128]{2,1,0:T(8,128)(2,1)S(1)} %all_to_all.16.received, bf16[512,256]{1,0:T(8,128)(2,1)S(1)} %get-tuple-element.40.matrix), custom_call_target="tpu_custom_call" | custom-call | tf_op jit(solution)/shard_map/output/pallas_call | solution.py:475
  38.7 6.8 %all-to-all-start.2 = ((bf16[8,40,256]{2,1,0:T(8,128)(2,1)}), bf16[8,40,256]{2,1,0:T(8,128)(2,1)S(1)}, u32[]{:S(2)}, u32[]{:S(2)}) async-start(bf16[8,40,256]{2,1,0:T(8,128)(2,1)} %output.1), calls=%async_computation.2 | async-start | bytes 327680 | tf_op jit(solution)/shard_map/all_to_all | solution.py:350
  45.5 3.0 %states.1 = (f32[4,6,8,64,128]{4,3,2,1,0:T(8,128)}, bf16[4,8,512]{2,1,0:T(8,128)(2,1)}, bf16[4,8,128]{2,1,0:T(8,128)(2,1)}, bf16[4,8,128]{2,1,0:T(8,128)(2,1)}) custom-call(f32[4,8,64,128]{3,2,1,0:T(8,128)S(1)} %get-tuple-element.28.carried, bf16[32,768]{1,0:T(8,128)(2,1)S(1)} %get-tuple-element.41.windows, f32[32,512]{1,0:T(8,128)S(1)} %get-tuple-element.42.step_x, ...), custom_call_target="tpu_custom_call" | custom-call | flops 200000000 | bytes 8000000 | tf_op jit(solution)/shard_map/states/pallas_call | solution.py:454
  48.5 2.6 %all-to-all-done.2.received = bf16[8,40,256]{2,1,0:T(8,128)(2,1)S(1)} async-done(((bf16[8,40,256]{2,1,0:T(8,128)(2,1)}), bf16[8,40,256]{2,1,0:T(8,128)(2,1)S(1)}, u32[]{:S(2)}, u32[]{:S(2)}) %all-to-all-start.2) | async-done | bytes 163872 | tf_op jit(solution)/shard_map/all_to_all | solution.py:350
  51.1 0.6 %total.1 = bf16[40,256]{1,0:T(8,128)(2,1)} custom-call(bf16[8,40,256]{2,1,0:T(8,128)(2,1)S(1)} %all-to-all-done.2.received), custom_call_target="tpu_custom_call" | custom-call | tf_op jit(solution)/shard_map/total/pallas_call | solution.py:483
Async XLA Ops:
  38.7 12.4 %all-to-all-start.2 = ((bf16[8,40,256]{2,1,0:T(8,128)(2,1)}), bf16[8,40,256]{2,1,0:T(8,128)(2,1)S(1)}, u32[]{:S(2)}, u32[]{:S(2)}) async-start(bf16[8,40,256]{2,1,0:T(8,128)(2,1)} %output.1), calls=%async_computation.2 | async-start | bytes 327680 | tf_op jit(solution)/shard_map/all_to_all | solution.py:350
